TPU v7x, 128 devices: a whole 4x4x4 slice. The times are simulated.
128 devices in a mesh: ep: 32 (over z, y, core), tp: 4 (over x).
Axes of the slice: x: 4, y: 4, z: 4, core: 2. Of those that a mesh axis runs over, the one named last changes fastest.
Arguments:
- query_rows: bfloat16 [16384, 2048], P('ep', 'tp'), may hold values from -6 to 6
- key_rows: bfloat16 [16384, 512], P('ep', 'tp'), may hold values from -6 to 6
- value_rows: bfloat16 [16384, 512], P('ep', 'tp'), may hold values from -6 to 6
- query_gain: float32 [64], replicated, may hold values from 0.2 to 4.5
- key_gain: float32 [64], replicated, may hold values from 0.2 to 4.5
- sink_logit: float32 [32], P('tp'), may hold values from 2 to 6
- out_weight: bfloat16 [2048, 2048], P('tp'), may hold values from -0.125 to 0.125
- tokens: bfloat16 [16384, 2048], P('ep'), may hold values from -6 to 6
- norm_gain: float32 [2048], replicated, may hold values from 0.1 to 1.9
- expert_ids: int32 [16384, 2], P('ep'), may hold values from 0 to 127, all different within a row; in each aligned block of 128 rows (0 to 127, 128 to 255, ...) at most 4 rows name the same one
- route_weight: float32 [16384, 2], P('ep'), may hold values from 0.2 to 1
- gate_weight: bfloat16 [128, 2048, 1024], P('ep', None, 'tp'), may hold values from -0.125 to 0.125
- up_weight: bfloat16 [128, 2048, 1024], P('ep', None, 'tp'), may hold values from -0.125 to 0.125
- down_weight: bfloat16 [128, 1024, 2048], P('ep', 'tp'), may hold values from -0.1875 to 0.1875
- shared_gate: bfloat16 [2048, 1024], P(None, 'tp'), may hold values from -0.125 to 0.125
- shared_up: bfloat16 [2048, 1024], P(None, 'tp'), may hold values from -0.125 to 0.125
- shared_down: bfloat16 [1024, 2048], P('tp'), may hold values from -0.1875 to 0.1875
Outputs:
- mixer_out: bfloat16 [16384, 2048], P(('ep', 'tp'))
- expert_out: bfloat16 [16384, 2048], P(('ep', 'tp'))
Inputs may be any that keep to these rules, and one draw needn't show every extreme that they name: `expert_ids`: each row names 2 different experts. In each aligned block of 128 rows no expert is named by more than 4 rows, a bound that some block reaches.
All inputs are finite; a program needn't handle non-finite values.
Results may differ from a plain program's by a relative error of at most 0.012.
The roundings to bfloat16 on the way count: a program that leaves them out, or rounds other values in their place, can miss the bound.
Values may be sent and summed in bfloat16 or wider, within the bound.
A program may use at most 128 MiB of HBM per device.

v0:
```python
import jax
import jax.numpy as jnp
from jax import lax
from jax.experimental import pallas as pl
from jax.experimental.pallas import tpu as pltpu
from jax.sharding import Mesh
from jax.sharding import PartitionSpec as P

HEADS = 32
KV_HEADS = 8
HEAD_DIM = 64
BLOCK = 128
CAP = 4
N_TP = 4
NZ, NY, NC = 4, 4, 2
N_EP = NZ * NY * NC
EP = ("z", "y", "c")
EP_TP = ("z", "y", "c", "x")
D = 2048
ROWS = 512
FFS = 256
EXPERTS = 128
LOCAL = 4
COLS = D // N_TP
SLOTS = N_EP * 16
EPS = 1e-06
MASKED = -1e30
MESH_ID = pl.DeviceIdType.MESH
BF = jnp.bfloat16
F32 = jnp.float32

PAIRS = (
    (0, 1), (1, 0), (0, 3), (3, 0), (1, 2), (2, 1), (3, 2), (2, 3),
    (1, 1), (3, 3), (1, 3), (3, 1), (2, 0), (0, 2), (2, 2), (0, 0),
)
PEERS = tuple((dz, dy, dc) for dc in range(2) for dz, dy in PAIRS if (dz, dy, dc) != (0, 0, 0))


def dot(a, b):
    return jnp.dot(a, b, preferred_element_type=F32)


def layer_kernel(
    q_ref, k_ref, v_ref, qg_ref, kg_ref, sink_ref, gain_ref, ids_ref, rw_ref,
    tok_hbm, ow_hbm, wg_hbm, wu_hbm, wd_hbm, sg_hbm, su_hbm, sd_hbm,
    mix_out, exp_out,
    normed, ow, wg, wu, wd, sg, su, sd,
    slots, disp_send, disp_recv, rs_recv, ret_send, ret_recv,
    mix_send, mix_recv, sh_send, sh_recv, acc, fin_send, fin_recv,
    halo, kd, vd, heads,
    load_sem, dsend, drecv, rsend, rrecv, tsend, trecv,
    msend, mrecv, ssend, srecv, fsend, frecv, hsend, hrecv,
):
    z, y, c, x = (lax.axis_index(a) for a in EP_TP)
    me = (z * NY + y) * NC + c

    def ep_peer(off):
        dz, dy, dc = off
        pz, py, pc = lax.rem(z + dz, NZ), lax.rem(y + dy, NY), lax.rem(c + dc, NC)
        return (pz, py, pc, x), (pz * NY + py) * NC + pc

    def x_peer(d):
        px = lax.rem(x + d, N_TP)
        return (z, y, c, px), px

    barrier = pltpu.get_barrier_semaphore()
    for off in PEERS:
        pl.semaphore_signal(barrier, inc=1, device_id=ep_peer(off)[0], device_id_type=MESH_ID)
    for d in range(1, N_TP):
        pl.semaphore_signal(barrier, inc=1, device_id=x_peer(d)[0], device_id_type=MESH_ID)

    loads = [
        pltpu.make_async_copy(s, t, load_sem.at[i])
        for i, (s, t) in enumerate(
            [(tok_hbm, normed), (ow_hbm, ow), (sg_hbm, sg), (su_hbm, su), (sd_hbm, sd),
             (wg_hbm, wg), (wu_hbm, wu), (wd_hbm, wd)]
        )
    ]
    for cp in loads:
        cp.start()

    ids = ids_ref[...]
    expert = lax.broadcasted_iota(jnp.int32, (EXPERTS, ROWS), 0)
    first = (expert == ids[0:1, :]).astype(F32)
    second = (expert == ids[1:2, :]).astype(F32)
    s_row = lax.broadcasted_iota(jnp.int32, (ROWS, ROWS), 0)
    s_col = lax.broadcasted_iota(jnp.int32, (ROWS, ROWS), 1)
    earlier = ((s_row < s_col) & ((s_row >> 7) == (s_col >> 7))).astype(F32).astype(BF)
    seen = dot((first + second).astype(BF), earlier)
    rank_a = jnp.sum(first * seen, axis=0, keepdims=True)
    rank_b = jnp.sum(second * seen, axis=0, keepdims=True)
    place = (ids & 3) * SLOTS + (ids >> 2) * 16
    place = place + (lax.broadcasted_iota(jnp.int32, (2, ROWS), 1) >> 7) * CAP
    slots[0:1, :] = place[0:1, :].astype(F32) + rank_a
    slots[1:2, :] = place[1:2, :].astype(F32) + rank_b

    loads[0].wait()

    def norm_step(i, carry):
        rows = pl.ds(pl.multiple_of(i * 64, 64), 64)
        wide = normed[rows, :].astype(F32)
        scale = lax.rsqrt(jnp.mean(wide * wide, axis=-1, keepdims=True) + EPS)
        normed[rows, :] = ((wide * scale) * gain_ref[...]).astype(BF)
        return carry

    lax.fori_loop(0, ROWS // 64, norm_step, 0)

    mine = pl.ds(pl.multiple_of(me * 16, 16), 16)

    def slot_rows(j):
        index = lax.broadcasted_iota(jnp.int32, (SLOTS, ROWS), 0) + j * SLOTS
        return index.astype(F32)

    def send_chunk(j):
        for off in PEERS:
            dev, who = ep_peer(off)
            pltpu.make_async_remote_copy(
                src_ref=disp_send.at[j, pl.ds(pl.multiple_of(who * 16, 16), 16)],
                dst_ref=disp_recv.at[j, mine],
                send_sem=dsend.at[j], recv_sem=drecv.at[j],
                device_id=dev, device_id_type=MESH_ID,
            ).start()

    def whole_chunk(j):
        return pltpu.make_async_remote_copy(
            src_ref=disp_send.at[j, pl.ds(0, SLOTS - 16)],
            dst_ref=disp_recv.at[j, pl.ds(0, SLOTS - 16)],
            send_sem=dsend.at[j], recv_sem=drecv.at[j],
            device_id=ep_peer(PEERS[0])[0], device_id_type=MESH_ID,
        )

    def gather_step(j, carry):
        index = slot_rows(j)
        pick = (index == slots[0:1, :]) | (index == slots[1:2, :])
        pick = pick.astype(F32).astype(BF)
        for n in range(N_TP):
            cols = slice(n * COLS, (n + 1) * COLS)
            disp_send[j, :, cols] = dot(pick, normed[:, cols]).astype(BF)

        @pl.when(j == 0)
        def _():
            pl.semaphore_wait(barrier, len(PEERS) + N_TP - 1)

        @pl.when(j < 2)
        def _():
            send_chunk(j)

        disp_recv[j, mine, :] = disp_send[j, mine, :]
        return carry

    lax.fori_loop(0, LOCAL, gather_step, 0)

    nxt = lax.rem(me + 1, N_EP)
    nxt_dev = (nxt // (NY * NC), lax.rem(nxt // NC, NY), lax.rem(nxt, NC), x)
    halos = [
        pltpu.make_async_remote_copy(
            src_ref=ref.at[pl.ds(ROWS - BLOCK, BLOCK)], dst_ref=halo.at[i],
            send_sem=hsend.at[i], recv_sem=hrecv.at[i],
            device_id=nxt_dev, device_id_type=MESH_ID,
        )
        for i, ref in enumerate((k_ref, v_ref))
    ]
    for cp in halos:
        cp.start()

    loads[2].wait()
    loads[3].wait()
    loads[4].wait()
    gate = dot(normed[...], sg[...])
    up = dot(normed[...], su[...])
    hidden = (gate / (1.0 + jnp.exp(-gate)) * up).astype(BF)
    for n in range(N_TP):
        cols = slice(n * COLS, (n + 1) * COLS)
        sh_send[:, cols] = dot(hidden, sd[:, cols]).astype(BF)

    def col_block(px):
        return pl.ds(pl.multiple_of(px * COLS, COLS), COLS)

    def shared_copies():
        out = []
        for d in range(1, N_TP):
            dev, px = x_peer(d)
            out.append(pltpu.make_async_remote_copy(
                src_ref=sh_send.at[:, col_block(px)], dst_ref=sh_recv.at[d - 1],
                send_sem=ssend.at[d - 1], recv_sem=srecv.at[d - 1],
                device_id=dev, device_id_type=MESH_ID,
            ))
        return out

    lane = lax.broadcasted_iota(jnp.int32, (1, 128), 1)
    low = lane < HEAD_DIM
    half_a = lax.broadcasted_iota(jnp.int32, (128, 128), 0) >> 6
    half_b = lax.broadcasted_iota(jnp.int32, (128, 128), 1) >> 6
    same_half = (half_a == half_b).astype(F32).astype(BF)

    def head_norm(rows_in, gain):
        wide = rows_in.astype(F32)
        square = wide * wide
        top = square.astype(BF)
        rest = (square - top.astype(F32)).astype(BF)
        total = dot(top, same_half) + dot(rest, same_half)
        scale = lax.rsqrt(total * (1.0 / HEAD_DIM) + EPS)
        return ((wide * scale) * gain).astype(BF)

    def both_halves(rows_in, dst, rows):
        wide = rows_in.astype(F32)
        turned = pltpu.roll(wide, HEAD_DIM, 1)
        dst[0, rows, :] = jnp.where(low, wide, turned).astype(BF)
        dst[1, rows, :] = jnp.where(low, turned, wide).astype(BF)

    own_rows = slice(BLOCK, BLOCK + ROWS)
    both_halves(head_norm(k_ref[...], kg_ref[...]), kd, own_rows)
    both_halves(v_ref[...], vd, own_rows)
    for cp in halos:
        cp.wait()
    both_halves(head_norm(halo[0], kg_ref[...]), kd, slice(0, BLOCK))
    both_halves(halo[1], vd, slice(0, BLOCK))
    query_pos = lax.broadcasted_iota(jnp.int32, (BLOCK, 2 * BLOCK), 0)
    key_pos = lax.broadcasted_iota(jnp.int32, (BLOCK, 2 * BLOCK), 1)

    def attend(n, carry):
        rows = pl.ds(pl.multiple_of(n * BLOCK, BLOCK), BLOCK)
        band = pl.ds(pl.multiple_of(n * BLOCK, BLOCK), 2 * BLOCK)
        floor = jnp.where(me * 4 + n == 0, BLOCK, 0)
        inside = (key_pos <= query_pos + BLOCK) & (key_pos > query_pos) & (key_pos >= floor)
        for kv in range(2):
            parts = []
            for b in range(2):
                cols = slice((kv * 2 + b) * 128, (kv * 2 + b + 1) * 128)
                qn = head_norm(q_ref[rows, cols], qg_ref[...]).astype(F32)
                parts.append(jnp.where(low, qn, 0.0).astype(BF))
                parts.append(jnp.where(low, 0.0, qn).astype(BF))
            stacked = jnp.concatenate(parts, axis=0)
            scores = lax.dot_general(
                stacked, kd[kv, band, :], (((1,), (1,)), ((), ())), preferred_element_type=F32
            ) * 0.125
            probs = []
            for g in range(4):
                sink = sink_ref[0, kv * 4 + g]
                part = jnp.where(inside, scores[g * BLOCK:(g + 1) * BLOCK], MASKED)
                top = jnp.maximum(jnp.max(part, axis=-1, keepdims=True), sink)
                ex = jnp.exp(part - top)
                den = jnp.sum(ex, axis=-1, keepdims=True) + jnp.exp(sink - top)
                probs.append((ex * (1.0 / den)).astype(BF))
            mixed = dot(jnp.concatenate(probs, axis=0), vd[kv, band, :])
            for b in range(2):
                lo = mixed[(2 * b) * BLOCK:(2 * b + 1) * BLOCK]
                hi = mixed[(2 * b + 1) * BLOCK:(2 * b + 2) * BLOCK]
                cols = slice((kv * 2 + b) * 128, (kv * 2 + b + 1) * 128)
                heads[rows, cols] = jnp.where(low, lo, hi).astype(BF)
        return carry

    for cp in shared_copies():
        cp.start()

    lax.fori_loop(0, ROWS // BLOCK, attend, 0)
    loads[1].wait()
    for n in range(N_TP):
        cols = slice(n * COLS, (n + 1) * COLS)
        mix_send[:, cols] = dot(heads[...], ow[:, cols]).astype(BF)

    def quarter(px):
        return pl.ds(pl.multiple_of(px * BLOCK, BLOCK), BLOCK)

    def mixer_copies():
        out = []
        for d in range(1, N_TP):
            dev, px = x_peer(d)
            out.append(pltpu.make_async_remote_copy(
                src_ref=mix_send.at[quarter(px)], dst_ref=mix_recv.at[d - 1],
                send_sem=msend.at[d - 1], recv_sem=mrecv.at[d - 1],
                device_id=dev, device_id_type=MESH_ID,
            ))
        return out

    for cp in mixer_copies():
        cp.start()

    loads[5].wait()
    loads[6].wait()
    loads[7].wait()

    def rs_copies(j):
        out = []
        for d in range(1, N_TP):
            dev, px = x_peer(d)
            out.append(pltpu.make_async_remote_copy(
                src_ref=disp_send.at[j, :, col_block(px)], dst_ref=rs_recv.at[j, d - 1],
                send_sem=rsend.at[j, d - 1], recv_sem=rrecv.at[j, d - 1],
                device_id=dev, device_id_type=MESH_ID,
            ))
        return out

    def whole_return(j):
        return pltpu.make_async_remote_copy(
            src_ref=ret_send.at[j, pl.ds(0, SLOTS - 16)],
            dst_ref=ret_recv.at[j, pl.ds(0, SLOTS - 16)],
            send_sem=tsend.at[j], recv_sem=trecv.at[j],
            device_id=ep_peer(PEERS[0])[0], device_id_type=MESH_ID,
        )

    def step(i, carry):
        @pl.when(i < LOCAL)
        def _():
            whole_chunk(i).wait()

            @pl.when(i < 2)
            def _():
                send_chunk(i + 2)

            gate = dot(disp_recv[i], wg[i])
            up = dot(disp_recv[i], wu[i])
            hidden = (gate / (1.0 + jnp.exp(-gate)) * up).astype(BF)
            for n in range(N_TP):
                cols = slice(n * COLS, (n + 1) * COLS)
                disp_send[i, :, cols] = dot(hidden, wd[i, :, cols]).astype(BF)
            for cp in rs_copies(i):
                cp.start()

        @pl.when(i == LOCAL)
        def _():
            for cp in mixer_copies():
                cp.wait()
            total = mix_send[quarter(x), :].astype(F32)
            for d in range(N_TP - 1):
                total = total + mix_recv[d].astype(F32)
            mix_out[...] = total.astype(BF)

        @pl.when((i >= 1) & (i <= LOCAL))
        def _():
            j = i - 1
            for cp in rs_copies(j):
                cp.wait()
            total = disp_send[j, :, col_block(x)].astype(F32)
            for d in range(N_TP - 1):
                total = total + rs_recv[j, d].astype(F32)
            ret_send[j] = total.astype(BF)
            for off in PEERS:
                dev, who = ep_peer(off)
                pltpu.make_async_remote_copy(
                    src_ref=ret_send.at[j, pl.ds(pl.multiple_of(who * 16, 16), 16)],
                    dst_ref=ret_recv.at[j, mine],
                    send_sem=tsend.at[j], recv_sem=trecv.at[j],
                    device_id=dev, device_id_type=MESH_ID,
                ).start()
            ret_recv[j, mine, :] = ret_send[j, mine, :]

        @pl.when(i == 2)
        def _():
            for cp in shared_copies():
                cp.wait()
            total = sh_send[:, col_block(x)].astype(F32)
            for d in range(N_TP - 1):
                total = total + sh_recv[d].astype(F32)
            acc[...] = total.astype(BF).astype(F32)

        @pl.when(i >= 2)
        def _():
            j = i - 2
            whole_return(j).wait()
            index = slot_rows(j)
            weight = jnp.where(index == slots[0:1, :], rw_ref[0:1, :], 0.0)
            weight = weight + jnp.where(index == slots[1:2, :], rw_ref[1:2, :], 0.0)
            main = weight.astype(BF)
            rest = (weight - main.astype(F32)).astype(BF)
            dims = (((0,), (0,)), ((), ()))
            back = ret_recv[j]
            acc[...] += lax.dot_general(
                main, back, dims, preferred_element_type=F32
            ) + lax.dot_general(rest, back, dims, preferred_element_type=F32)

        return carry

    lax.fori_loop(0, LOCAL + 2, step, 0)

    fin_send[...] = acc[...].astype(BF)
    finals = []
    for d in range(1, N_TP):
        dev, px = x_peer(d)
        finals.append(pltpu.make_async_remote_copy(
            src_ref=fin_send.at[quarter(px)], dst_ref=fin_recv.at[d - 1],
            send_sem=fsend.at[d - 1], recv_sem=frecv.at[d - 1],
            device_id=dev, device_id_type=MESH_ID,
        ))
    for cp in finals:
        cp.start()
    exp_out[:, col_block(x)] = fin_send[quarter(x), :]
    for d, cp in enumerate(finals):
        cp.wait()
        exp_out[:, col_block(lax.rem(x + N_TP - 1 - d, N_TP))] = fin_recv[d]


def shards(
    query_rows, key_rows, value_rows, query_gain, key_gain, sink_logit, out_weight, tokens,
    norm_gain, expert_ids, route_weight, gate_weight, up_weight, down_weight,
    shared_gate, shared_up, shared_down,
):
    vmem = pl.BlockSpec(memory_space=pltpu.VMEM)
    hbm = pl.BlockSpec(memory_space=pl.ANY)
    smem = pl.BlockSpec(memory_space=pltpu.SMEM)
    dma = pltpu.SemaphoreType.DMA
    out = jax.ShapeDtypeStruct((BLOCK, D), BF)
    return pl.pallas_call(
        layer_kernel,
        out_shape=(out, out),
        in_specs=[vmem] * 5 + [smem] + [vmem] * 3 + [hbm] * 8,
        out_specs=(vmem, vmem),
        scratch_shapes=[
            pltpu.VMEM((ROWS, D), BF),
            pltpu.VMEM((ROWS, D), BF),
            pltpu.VMEM((LOCAL, D, FFS), BF),
            pltpu.VMEM((LOCAL, D, FFS), BF),
            pltpu.VMEM((LOCAL, FFS, D), BF),
            pltpu.VMEM((D, FFS), BF),
            pltpu.VMEM((D, FFS), BF),
            pltpu.VMEM((FFS, D), BF),
            pltpu.VMEM((2, ROWS), F32),
            pltpu.VMEM((LOCAL, SLOTS, D), BF),
            pltpu.VMEM((LOCAL, SLOTS, D), BF),
            pltpu.VMEM((LOCAL, N_TP - 1, SLOTS, COLS), BF),
            pltpu.VMEM((LOCAL, SLOTS, COLS), BF),
            pltpu.VMEM((LOCAL, SLOTS, COLS), BF),
            pltpu.VMEM((ROWS, D), BF),
            pltpu.VMEM((N_TP - 1, BLOCK, D), BF),
            pltpu.VMEM((ROWS, D), BF),
            pltpu.VMEM((N_TP - 1, ROWS, COLS), BF),
            pltpu.VMEM((ROWS, COLS), F32),
            pltpu.VMEM((ROWS, COLS), BF),
            pltpu.VMEM((N_TP - 1, BLOCK, COLS), BF),
            pltpu.VMEM((2, BLOCK, 128), BF),
            pltpu.VMEM((2, BLOCK + ROWS, 128), BF),
            pltpu.VMEM((2, BLOCK + ROWS, 128), BF),
            pltpu.VMEM((ROWS, 512), BF),
            dma((8,)),
            dma((LOCAL,)), dma((LOCAL,)),
            dma((LOCAL, N_TP - 1)), dma((LOCAL, N_TP - 1)),
            dma((LOCAL,)), dma((LOCAL,)),
            dma((N_TP - 1,)), dma((N_TP - 1,)),
            dma((N_TP - 1,)), dma((N_TP - 1,)),
            dma((N_TP - 1,)), dma((N_TP - 1,)),
            dma((2,)), dma((2,)),
        ],
        compiler_params=pltpu.CompilerParams(
            collective_id=0, has_side_effects=True, vmem_limit_bytes=67000000
        ),
        name="layer",
    )(
        query_rows, key_rows, value_rows,
        jnp.tile(query_gain, 2)[None], jnp.tile(key_gain, 2)[None],
        sink_logit[None], norm_gain[None], expert_ids.T, route_weight.T,
        tokens, out_weight, gate_weight, up_weight, down_weight,
        shared_gate, shared_up, shared_down,
    )


def solution(mesh):
    split = Mesh(mesh.devices.reshape(NZ, NY, NC, mesh.shape["tp"]), EP_TP)
    return jax.shard_map(
        shards,
        mesh=split,
        in_specs=(
            P(EP, "x"), P(EP, "x"), P(EP, "x"), P(), P(), P("x"), P("x", None),
            P(EP, None), P(), P(EP, None), P(EP, None),
            P(EP, None, "x"), P(EP, None, "x"), P(EP, "x", None),
            P(None, "x"), P(None, "x"), P("x", None),
        ),
        out_specs=(P(EP_TP, None), P(EP_TP, None)),
        check_vma=False,
    )
```

profile of v0, /device:TPU:1, one launch (start us, length us, event | category | flops | bytes accessed | tf_op | source)
XLA Modules:
  0.0 219.3 jit_solution(7603137087888035007)
XLA Ops:
  0.6 0.7 tile.4
  1.3 0.6 broadcast_in_dim_tile.6.qg_ref
  1.9 0.7 tile.5
  2.5 0.6 broadcast_in_dim_tile.7.kg_ref
  3.1 212.4 %layer.1 = (bf16[128,2048]{1,0:T(8,128)(2,1)}, bf16[128,2048]{1,0:T(8,128)(2,1)}) custom-call(bf16[512,512]{1,0:T(8,128)(2,1)} %q_ref.1, bf16[512,128]{1,0:T(8,128)(2,1)} %k_ref.1, bf16[512,128]{1,0:T(8,128)(2,1)} %v_ref.1, f32[1,128]{1,0:T(1,128)} %broadcast_in_dim_tile.6.qg_ref, f32[1,128]{1,0:T(1,128)} %broadcast_in_dim_tile.7.kg_ref, f32[1,8]{1,0:T(1,128)} %bitcast.7, ...), custom_call_target="tpu_custom_call" | custom-call | tf_op jit(solution)/shard_map/layer/pallas_call | solution.py:403
  215.5 1.9 copy.21
  217.4 1.9 copy.22
where the time goes:
time: 220 us; the launch traced here: 219 us
  Pallas kernels  212 us (96%)
  local copies, waits for them, and re-layouts  6.26 us (3%)
    pallas_call x1, Pallas kernels, shards(): pl.pallas_call(layer_kernel, out_shape=(out, out), in_specs=[vmem] * 5 +...  212 us

commit v1 on v0

v1 whole, which is shorter than its diff:
```python
import jax
import jax.numpy as jnp
from jax import lax
from jax.experimental import pallas as pl
from jax.experimental.pallas import tpu as pltpu
from jax.sharding import Mesh
from jax.sharding import PartitionSpec as P

HEADS = 32
KV_HEADS = 8
HEAD_DIM = 64
BLOCK = 128
CAP = 4
N_TP = 4
NZ, NY, NC = 4, 4, 2
N_EP = NZ * NY * NC
EP = ("z", "y", "c")
EP_TP = ("z", "y", "c", "x")
D = 2048
ROWS = 512
FFS = 256
EXPERTS = 128
LOCAL = 4
COLS = D // N_TP
SLOTS = N_EP * 16
EPS = 1e-06
MASKED = -1e30
MESH_ID = pl.DeviceIdType.MESH
BF = jnp.bfloat16
F32 = jnp.float32

ORDER = tuple(((k + k // NY) % NZ) * NY + k % NY for k in range(NZ * NY))
HALVES = tuple(tuple(dc * NZ * NY + o for o in ORDER if (dc, o) != (0, 0)) for dc in range(NC))
PEERS = HALVES[0] + HALVES[1]
HALF = SLOTS // 2


def dot(a, b):
    return jnp.dot(a, b, preferred_element_type=F32)


def layer_kernel(
    q_ref, k_ref, v_ref, qg_ref, kg_ref, sink_ref, gain_ref, ids_ref, rw_ref,
    tok_hbm, ow_hbm, wg_hbm, wu_hbm, wd_hbm, sg_hbm, su_hbm, sd_hbm,
    mix_out, exp_out,
    normed, ow, wg, wu, wd, sg, su, sd,
    slots, disp_send, disp_recv, rs_relay, rs_side, ret_send, ret_recv,
    mix_send, mix_relay, mix_side, sh_send, sh_relay, sh_side, acc, fin_send, fin_recv,
    halo, kd, vd, heads,
    load_sem, dsend, drecv, xsend, xrecv, tsend, trecv, fsend, frecv, hsend, hrecv,
):
    z, y, c, x = (lax.axis_index(a) for a in EP_TP)
    me = (z * NY + y) * NC + c

    def ep_peer(slot, sign=1):
        dc, dz, dy = slot // (NZ * NY), slot // NY % NZ, slot % NY
        return (
            lax.rem(z + (dz * sign) % NZ, NZ), lax.rem(y + (dy * sign) % NY, NY),
            lax.rem(c + dc, NC), x,
        )

    def x_peer(d):
        return (z, y, c, lax.rem(x + d % N_TP, N_TP))

    barrier = pltpu.get_barrier_semaphore()
    for slot in PEERS:
        pl.semaphore_signal(barrier, inc=1, device_id=ep_peer(slot), device_id_type=MESH_ID)
    for d in range(1, N_TP):
        pl.semaphore_signal(barrier, inc=1, device_id=x_peer(d), device_id_type=MESH_ID)

    loads = [
        pltpu.make_async_copy(s, t, load_sem.at[i])
        for i, (s, t) in enumerate(
            [(tok_hbm, normed), (ow_hbm, ow), (sg_hbm, sg), (su_hbm, su), (sd_hbm, sd),
             (wg_hbm, wg), (wu_hbm, wu), (wd_hbm, wd)]
        )
    ]
    for cp in loads:
        cp.start()

    ids = ids_ref[...]
    expert = lax.broadcasted_iota(jnp.int32, (EXPERTS, ROWS), 0)
    first = (expert == ids[0:1, :]).astype(F32)
    second = (expert == ids[1:2, :]).astype(F32)
    s_row = lax.broadcasted_iota(jnp.int32, (ROWS, ROWS), 0)
    s_col = lax.broadcasted_iota(jnp.int32, (ROWS, ROWS), 1)
    earlier = ((s_row < s_col) & ((s_row >> 7) == (s_col >> 7))).astype(F32).astype(BF)
    seen = dot((first + second).astype(BF), earlier)
    rank_a = jnp.sum(first * seen, axis=0, keepdims=True)
    rank_b = jnp.sum(second * seen, axis=0, keepdims=True)
    owner = ids >> 2
    away = ((owner ^ c) & 1) * NZ * NY + (((owner >> 3) - z) & 3) * NY + (((owner >> 1) - y) & 3)
    place = (ids & 3) * SLOTS + away * 16
    place = place + (lax.broadcasted_iota(jnp.int32, (2, ROWS), 1) >> 7) * CAP
    slots[0:1, :] = place[0:1, :].astype(F32) + rank_a
    slots[1:2, :] = place[1:2, :].astype(F32) + rank_b

    with jax.named_scope('wait_tokens'):
        loads[0].wait()

    def norm_step(i, carry):
        rows = pl.ds(pl.multiple_of(i * 64, 64), 64)
        wide = normed[rows, :].astype(F32)
        scale = lax.rsqrt(jnp.mean(wide * wide, axis=-1, keepdims=True) + EPS)
        normed[rows, :] = ((wide * scale) * gain_ref[...]).astype(BF)
        return carry

    with jax.named_scope('norm'):
        lax.fori_loop(0, ROWS // 64, norm_step, 0)

    def slot_rows(base, rows):
        index = lax.broadcasted_iota(jnp.int32, (rows, ROWS), 0) + base
        return index.astype(F32)

    def send_half(buf, to, half, j, send_sem, recv_sem, sign):
        for slot in HALVES[half]:
            rows = pl.ds(slot * 16, 16)
            pltpu.make_async_remote_copy(
                src_ref=buf.at[j, rows], dst_ref=to.at[j, rows],
                send_sem=send_sem.at[2 * j + half], recv_sem=recv_sem.at[2 * j + half],
                device_id=ep_peer(slot, sign), device_id_type=MESH_ID,
            ).start()

    def wait_half(buf, to, h, send_sem, recv_sem):
        for half in range(2):
            @pl.when(lax.rem(h, 2) == half)
            def _():
                rows = pl.ds(0, len(HALVES[half]) * 16)
                pltpu.make_async_remote_copy(
                    src_ref=buf.at[h // 2, rows], dst_ref=to.at[h // 2, rows],
                    send_sem=send_sem.at[h], recv_sem=recv_sem.at[h],
                    device_id=ep_peer(1), device_id_type=MESH_ID,
                ).wait()

    nxt = lax.rem(me + 1, N_EP)
    nxt_dev = (nxt // (NY * NC), lax.rem(nxt // NC, NY), lax.rem(nxt, NC), x)
    halos = [
        pltpu.make_async_remote_copy(
            src_ref=ref.at[pl.ds(ROWS - BLOCK, BLOCK)], dst_ref=halo.at[i],
            send_sem=hsend.at[i], recv_sem=hrecv.at[i],
            device_id=nxt_dev, device_id_type=MESH_ID,
        )
        for i, ref in enumerate((k_ref, v_ref))
    ]

    def gather_step(j, carry):
        index = slot_rows(j * SLOTS, SLOTS)
        pick = (index == slots[0:1, :]) | (index == slots[1:2, :])
        pick = pick.astype(F32).astype(BF)
        for n in range(N_TP):
            cols = slice(n * COLS, (n + 1) * COLS)
            disp_send[j, :, cols] = dot(pick, normed[:, cols]).astype(BF)

        @pl.when(j == 0)
        def _():
            with jax.named_scope('barrier'):
                pl.semaphore_wait(barrier, len(PEERS) + N_TP - 1)
            for cp in halos:
                cp.start()

        with jax.named_scope('send'):
            for half in range(2):
                send_half(disp_send, disp_recv, half, j, dsend, drecv, 1)
        disp_recv[j, 0:16, :] = disp_send[j, 0:16, :]
        return carry

    with jax.named_scope('gather'):
        lax.fori_loop(0, LOCAL, gather_step, 0)

    def x_copy(t, n, src, dst, d):
        return pltpu.make_async_remote_copy(
            src_ref=src, dst_ref=dst, send_sem=xsend.at[t, n], recv_sem=xrecv.at[t, n],
            device_id=x_peer(d), device_id_type=MESH_ID,
        )

    def x_copies(which, t, part, relay, sides):
        routes = (
            (part(2, 0), relay(0), 1),
            (part(2, 1), relay(1), -1),
            (part(1, 1), sides(0, 1), 1),
            (part(-1, 0), sides(1, 0), -1),
            (part(1, 0), sides(0, 0), 1),
            (part(-1, 1), sides(1, 1), -1),
        )
        return [x_copy(t, n, *routes[n]) for n in which]

    def start_first(*refs):
        for cp in x_copies((0, 1, 2, 3), *refs):
            cp.start()

    def start_second(t, part, relay, sides):
        for cp in x_copies((0, 1), t, part, relay, sides):
            cp.wait()
        for n, d in ((0, 1), (1, -1)):
            own = part(d, n)
            own[...] = (own[...].astype(F32) + relay(n)[...].astype(F32)).astype(BF)
        for cp in x_copies((4, 5), t, part, relay, sides):
            cp.start()

    def wait_rest(*refs):
        for cp in x_copies((2, 3, 4, 5), *refs):
            cp.wait()

    def summed(t, part, relay, sides, half):
        return (
            part(0, half)[...].astype(F32)
            + sides(0, half)[...].astype(F32) + sides(1, half)[...].astype(F32)
        )

    def col_block(d):
        return pl.ds(pl.multiple_of(lax.rem(x + d % N_TP, N_TP) * COLS, COLS), COLS)

    def shared_refs():
        half = ROWS // 2
        return (
            2 * LOCAL,
            lambda d, n: sh_send.at[pl.ds(n * half, half), col_block(d)],
            lambda n: sh_relay.at[n],
            lambda s, n: sh_side.at[s, pl.ds(n * half, half)],
        )

    def mixer_refs():
        half = BLOCK // 2

        def part(d, n):
            at = lax.rem(x + d % N_TP, N_TP) * BLOCK + n * half
            return mix_send.at[pl.ds(pl.multiple_of(at, half), half)]

        return (
            2 * LOCAL + 1, part, lambda n: mix_relay.at[n],
            lambda s, n: mix_side.at[s, pl.ds(n * half, half)],
        )

    def expert_refs(h):
        half = HALF // 2
        j, base = h // 2, lax.rem(h, 2) * HALF

        def part(d, n):
            at = pl.multiple_of(base + n * half, half)
            return disp_send.at[j, pl.ds(at, half), col_block(d)]

        return (
            h, part, lambda n: rs_relay.at[h, n],
            lambda s, n: rs_side.at[h, s, pl.ds(n * half, half)],
        )

    loads[2].wait()
    loads[3].wait()
    loads[4].wait()
    gate = dot(normed[...], sg[...])
    up = dot(normed[...], su[...])
    hidden = (gate / (1.0 + jnp.exp(-gate)) * up).astype(BF)
    for n in range(N_TP):
        cols = slice(n * COLS, (n + 1) * COLS)
        sh_send[:, cols] = dot(hidden, sd[:, cols]).astype(BF)

    start_first(*shared_refs())

    lane = lax.broadcasted_iota(jnp.int32, (1, 128), 1)
    low = lane < HEAD_DIM
    half_a = lax.broadcasted_iota(jnp.int32, (128, 128), 0) >> 6
    half_b = lax.broadcasted_iota(jnp.int32, (128, 128), 1) >> 6
    same_half = (half_a == half_b).astype(F32).astype(BF)

    q_gain = jnp.concatenate([qg_ref[...], qg_ref[...]], axis=1)
    k_gain = jnp.concatenate([kg_ref[...], kg_ref[...]], axis=1)

    def head_norm(rows_in, gain):
        wide = rows_in.astype(F32)
        square = wide * wide
        top = square.astype(BF)
        rest = (square - top.astype(F32)).astype(BF)
        total = dot(top, same_half) + dot(rest, same_half)
        scale = lax.rsqrt(total * (1.0 / HEAD_DIM) + EPS)
        return ((wide * scale) * gain).astype(BF)

    def both_halves(rows_in, dst, rows):
        wide = rows_in.astype(F32)
        turned = pltpu.roll(wide, HEAD_DIM, 1)
        dst[0, rows, :] = jnp.where(low, wide, turned).astype(BF)
        dst[1, rows, :] = jnp.where(low, turned, wide).astype(BF)

    own_rows = slice(BLOCK, BLOCK + ROWS)
    both_halves(head_norm(k_ref[...], k_gain), kd, own_rows)
    both_halves(v_ref[...], vd, own_rows)
    with jax.named_scope('halo_wait'):
        for cp in halos:
            cp.wait()
    both_halves(head_norm(halo[0], k_gain), kd, slice(0, BLOCK))
    both_halves(halo[1], vd, slice(0, BLOCK))
    query_pos = lax.broadcasted_iota(jnp.int32, (BLOCK, 2 * BLOCK), 0)
    key_pos = lax.broadcasted_iota(jnp.int32, (BLOCK, 2 * BLOCK), 1)

    def attend(n, carry):
        rows = pl.ds(pl.multiple_of(n * BLOCK, BLOCK), BLOCK)
        band = pl.ds(pl.multiple_of(n * BLOCK, BLOCK), 2 * BLOCK)
        floor = jnp.where(me * 4 + n == 0, BLOCK, 0)
        inside = (key_pos <= query_pos + BLOCK) & (key_pos > query_pos) & (key_pos >= floor)
        for kv in range(2):
            parts = []
            for b in range(2):
                cols = slice((kv * 2 + b) * 128, (kv * 2 + b + 1) * 128)
                qn = head_norm(q_ref[rows, cols], q_gain).astype(F32)
                parts.append(jnp.where(low, qn, 0.0).astype(BF))
                parts.append(jnp.where(low, 0.0, qn).astype(BF))
            stacked = jnp.concatenate(parts, axis=0)
            scores = lax.dot_general(
                stacked, kd[kv, band, :], (((1,), (1,)), ((), ())), preferred_element_type=F32
            ) * 0.125
            probs = []
            for g in range(4):
                sink = sink_ref[0, kv * 4 + g]
                part = jnp.where(inside, scores[g * BLOCK:(g + 1) * BLOCK], MASKED)
                top = jnp.maximum(jnp.max(part, axis=-1, keepdims=True), sink)
                ex = jnp.exp(part - top)
                den = jnp.sum(ex, axis=-1, keepdims=True) + jnp.exp(sink - top)
                probs.append((ex * (1.0 / den)).astype(BF))
            mixed = dot(jnp.concatenate(probs, axis=0), vd[kv, band, :])
            for b in range(2):
                lo = mixed[(2 * b) * BLOCK:(2 * b + 1) * BLOCK]
                hi = mixed[(2 * b + 1) * BLOCK:(2 * b + 2) * BLOCK]
                cols = slice((kv * 2 + b) * 128, (kv * 2 + b + 1) * 128)
                heads[rows, cols] = jnp.where(low, lo, hi).astype(BF)
        return carry

    with jax.named_scope('attend'):
        lax.fori_loop(0, ROWS // BLOCK, attend, 0)
    loads[1].wait()
    for n in range(N_TP):
        cols = slice(n * COLS, (n + 1) * COLS)
        mix_send[:, cols] = dot(heads[...], ow[:, cols]).astype(BF)

    start_first(*mixer_refs())
    with jax.named_scope('shared2'):
        start_second(*shared_refs())

    loads[5].wait()
    loads[6].wait()
    loads[7].wait()

    def combine(h, carry):
        with jax.named_scope('wait_ret'):
            wait_half(ret_send, ret_recv, h, tsend, trecv)
        with jax.named_scope('combine'):
            index = slot_rows(h * HALF, HALF)
            weight = jnp.where(index == slots[0:1, :], rw_ref[0:1, :], 0.0)
            weight = weight + jnp.where(index == slots[1:2, :], rw_ref[1:2, :], 0.0)
            main = weight.astype(BF)
            rest = (weight - main.astype(F32)).astype(BF)
            dims = (((0,), (0,)), ((), ()))
            back = ret_recv[h // 2, pl.ds(pl.multiple_of(lax.rem(h, 2) * HALF, HALF), HALF), :]
            acc[...] += lax.dot_general(
                main, back, dims, preferred_element_type=F32
            ) + lax.dot_general(rest, back, dims, preferred_element_type=F32)
        return carry

    def step(i, carry):
        @pl.when(i < 2 * LOCAL)
        def _():
            with jax.named_scope('wait_disp'):
                wait_half(disp_send, disp_recv, i, dsend, drecv)
            j = i // 2
            rows = pl.ds(pl.multiple_of(lax.rem(i, 2) * HALF, HALF), HALF)
            with jax.named_scope('ffn'):
                came = disp_recv[j, rows, :]
                gate = dot(came, wg[j])
                up = dot(came, wu[j])
                hidden = (gate / (1.0 + jnp.exp(-gate)) * up).astype(BF)
                for n in range(N_TP):
                    cols = slice(n * COLS, (n + 1) * COLS)
                    disp_send[j, rows, cols] = dot(hidden, wd[j, :, cols]).astype(BF)
            start_first(*expert_refs(i))

        @pl.when(i == 2)
        def _():
            with jax.named_scope('mix2'):
                start_second(*mixer_refs())

        @pl.when((i >= 1) & (i <= 2 * LOCAL))
        def _():
            with jax.named_scope('rs2'):
                start_second(*expert_refs(i - 1))

        @pl.when(i == 2 * LOCAL)
        def _():
            with jax.named_scope('mix_out'):
                wait_rest(*mixer_refs())
                for half in range(2):
                    rows = slice(half * BLOCK // 2, (half + 1) * BLOCK // 2)
                    mix_out[rows, :] = summed(*mixer_refs(), half).astype(BF)

        @pl.when((i >= 2) & (i <= 2 * LOCAL + 1))
        def _():
            h = i - 2
            j, base = h // 2, lax.rem(h, 2) * HALF
            with jax.named_scope('wait_rs'):
                wait_rest(*expert_refs(h))
            with jax.named_scope('ret'):
                for half in range(2):
                    at = pl.multiple_of(base + half * HALF // 2, HALF // 2)
                    ret_send[j, pl.ds(at, HALF // 2), :] = summed(
                        *expert_refs(h), half
                    ).astype(BF)
                for half in range(2):
                    @pl.when(lax.rem(h, 2) == half)
                    def _():
                        send_half(ret_send, ret_recv, half, j, tsend, trecv, -1)

            @pl.when(lax.rem(h, 2) == 0)
            def _():
                ret_recv[j, 0:16, :] = ret_send[j, 0:16, :]

        @pl.when(i == 3)
        def _():
            with jax.named_scope('wait_shared'):
                wait_rest(*shared_refs())
            for half in range(2):
                rows = slice(half * ROWS // 2, (half + 1) * ROWS // 2)
                acc[rows, :] = summed(*shared_refs(), half).astype(BF).astype(F32)

        low_h = jnp.where(i < 2 * LOCAL, 0, jnp.where(i == 2 * LOCAL, 0, jnp.where(i == 2 * LOCAL + 1, 3, 7)))
        high_h = jnp.where(i < 2 * LOCAL, 0, jnp.where(i == 2 * LOCAL, 3, jnp.where(i == 2 * LOCAL + 1, 7, 8)))
        lax.fori_loop(low_h, high_h, combine, 0)
        return carry

    lax.fori_loop(0, 2 * LOCAL + 3, step, 0)

    def quarter(d):
        at = lax.rem(x + d % N_TP, N_TP) * BLOCK
        return pl.ds(pl.multiple_of(at, BLOCK), BLOCK)

    fin_send[...] = acc[...].astype(BF)
    finals = [
        pltpu.make_async_remote_copy(
            src_ref=fin_send.at[quarter(d)], dst_ref=fin_recv.at[d - 1],
            send_sem=fsend.at[d - 1], recv_sem=frecv.at[d - 1],
            device_id=x_peer(d), device_id_type=MESH_ID,
        )
        for d in range(1, N_TP)
    ]
    for cp in finals:
        cp.start()
    exp_out[:, col_block(0)] = fin_send[quarter(0), :]
    for d in (1, 3, 2):
        with jax.named_scope('wait_fin'):
            finals[d - 1].wait()
        exp_out[:, col_block(-d)] = fin_recv[d - 1]


def shards(
    query_rows, key_rows, value_rows, query_gain, key_gain, sink_logit, out_weight, tokens,
    norm_gain, expert_ids, route_weight, gate_weight, up_weight, down_weight,
    shared_gate, shared_up, shared_down,
):
    vmem = pl.BlockSpec(memory_space=pltpu.VMEM)
    hbm = pl.BlockSpec(memory_space=pl.ANY)
    smem = pl.BlockSpec(memory_space=pltpu.SMEM)
    dma = pltpu.SemaphoreType.DMA
    out = jax.ShapeDtypeStruct((BLOCK, D), BF)
    return pl.pallas_call(
        layer_kernel,
        out_shape=(out, out),
        in_specs=[vmem] * 5 + [smem] + [vmem] * 3 + [hbm] * 8,
        out_specs=(vmem, vmem),
        scratch_shapes=[
            pltpu.VMEM((ROWS, D), BF),
            pltpu.VMEM((ROWS, D), BF),
            pltpu.VMEM((LOCAL, D, FFS), BF),
            pltpu.VMEM((LOCAL, D, FFS), BF),
            pltpu.VMEM((LOCAL, FFS, D), BF),
            pltpu.VMEM((D, FFS), BF),
            pltpu.VMEM((D, FFS), BF),
            pltpu.VMEM((FFS, D), BF),
            pltpu.VMEM((2, ROWS), F32),
            pltpu.VMEM((LOCAL, SLOTS, D), BF),
            pltpu.VMEM((LOCAL, SLOTS, D), BF),
            pltpu.VMEM((2 * LOCAL, 2, HALF // 2, COLS), BF),
            pltpu.VMEM((2 * LOCAL, 2, HALF, COLS), BF),
            pltpu.VMEM((LOCAL, SLOTS, COLS), BF),
            pltpu.VMEM((LOCAL, SLOTS, COLS), BF),
            pltpu.VMEM((ROWS, D), BF),
            pltpu.VMEM((2, BLOCK // 2, D), BF),
            pltpu.VMEM((2, BLOCK, D), BF),
            pltpu.VMEM((ROWS, D), BF),
            pltpu.VMEM((2, ROWS // 2, COLS), BF),
            pltpu.VMEM((2, ROWS, COLS), BF),
            pltpu.VMEM((ROWS, COLS), F32),
            pltpu.VMEM((ROWS, COLS), BF),
            pltpu.VMEM((N_TP - 1, BLOCK, COLS), BF),
            pltpu.VMEM((2, BLOCK, 128), BF),
            pltpu.VMEM((2, BLOCK + ROWS, 128), BF),
            pltpu.VMEM((2, BLOCK + ROWS, 128), BF),
            pltpu.VMEM((ROWS, 512), BF),
            dma((8,)),
            dma((2 * LOCAL,)), dma((2 * LOCAL,)),
            dma((2 * LOCAL + 2, 6)), dma((2 * LOCAL + 2, 6)),
            dma((2 * LOCAL,)), dma((2 * LOCAL,)),
            dma((N_TP - 1,)), dma((N_TP - 1,)),
            dma((2,)), dma((2,)),
        ],
        compiler_params=pltpu.CompilerParams(
            collective_id=0, has_side_effects=True, vmem_limit_bytes=67000000
        ),
        name="layer",
    )(
        query_rows, key_rows, value_rows,
        query_gain[None], key_gain[None],
        sink_logit[None], norm_gain[None], expert_ids.T, route_weight.T,
        tokens, out_weight, gate_weight, up_weight, down_weight,
        shared_gate, shared_up, shared_down,
    )


def solution(mesh):
    split = Mesh(mesh.devices.reshape(NZ, NY, NC, mesh.shape["tp"]), EP_TP)
    return jax.shard_map(
        shards,
        mesh=split,
        in_specs=(
            P(EP, "x"), P(EP, "x"), P(EP, "x"), P(), P(), P("x"), P("x", None),
            P(EP, None), P(), P(EP, None), P(EP, None),
            P(EP, None, "x"), P(EP, None, "x"), P(EP, "x", None),
            P(None, "x"), P(None, "x"), P("x", None),
        ),
        out_specs=(P(EP_TP, None), P(EP_TP, None)),
        check_vma=False,
    )
```

time: 220 us -> 145 us (0.66)
  Pallas kernels: 212 us -> 140 us
  local copies, waits for them, and re-layouts: 6.26 us -> 3.76 us
    pallas_call x1, Pallas kernels: 212 us -> 140 us  [shards(): pl.pallas_call(layer_kernel, out_shape=(out, out), in_specs=[vmem] * 5 +...]
    another operation x4 -> x0, local copies, waits for them, and re-layouts: 2.5 us -> none  [the longest x2 1.25 us: shards(): jnp.tile(query_gain, 2)[None]]
where the time goes in v1:
time: 145 us
  Pallas kernels  140 us (97%)
  local copies, waits for them, and re-layouts  3.76 us (3%)
    pallas_call x1, Pallas kernels, shards(): pl.pallas_call(layer_kernel, out_shape=(out, out), in_specs=[vmem] * 5 +...  140 us
    unnamed x2, local copies, waits for them, and re-layouts  3.76 us

profile of v1, /device:TPU:1, one launch (start us, length us, event | category | flops | bytes accessed | tf_op | source)
XLA Modules:
  0.0 144.5 jit_solution(1733841565457158443)
XLA Ops:
  0.6 140.1 %layer.1 = (bf16[128,2048]{1,0:T(8,128)(2,1)}, bf16[128,2048]{1,0:T(8,128)(2,1)}) custom-call(bf16[512,512]{1,0:T(8,128)(2,1)} %q_ref.1, bf16[512,128]{1,0:T(8,128)(2,1)} %k_ref.1, bf16[512,128]{1,0:T(8,128)(2,1)} %v_ref.1, f32[1,64]{1,0:T(1,128)} %bitcast.9, f32[1,64]{1,0:T(1,128)} %bitcast.10, f32[1,8]{1,0:T(1,128)} %bitcast.11, f32[1,2048]{1,0:T(1,128)} %bitcast.6, ...), custom_call_target="tpu_custom_call" | custom-call | tf_op jit(solution)/shard_map/layer/pallas_call | solution.py:460
  140.8 1.9 %copy.21 = bf16[128,2048]{1,0:T(8,128)(2,1)} copy(bf16[128,2048]{1,0:T(8,128)(2,1)} %get-tuple-element.4) | data formatting | bytes 1048576
  142.6 1.9 %copy.22 = bf16[128,2048]{1,0:T(8,128)(2,1)} copy(bf16[128,2048]{1,0:T(8,128)(2,1)} %get-tuple-element.5) | data formatting | bytes 1048576

commit v2 on v1

v2 whole, which is shorter than its diff:
```python
import jax
import jax.numpy as jnp
from jax import lax
from jax.experimental import pallas as pl
from jax.experimental.pallas import tpu as pltpu
from jax.sharding import Mesh
from jax.sharding import PartitionSpec as P

HEADS = 32
KV_HEADS = 8
HEAD_DIM = 64
BLOCK = 128
CAP = 4
N_TP = 4
NZ, NY, NC = 4, 4, 2
N_EP = NZ * NY * NC
EP = ("z", "y", "c")
EP_TP = ("z", "y", "c", "x")
D = 2048
ROWS = 512
FFS = 256
EXPERTS = 128
LOCAL = 4
COLS = D // N_TP
EPS = 1e-06
MASKED = -1e30
MESH_ID = pl.DeviceIdType.MESH
BF = jnp.bfloat16
F32 = jnp.float32

CHUNKS = N_EP // 4
CHUNK = 4 * LOCAL * 16
QUARTER = CHUNK // N_TP


def dot(a, b):
    return jnp.dot(a, b, preferred_element_type=F32)


def layer_kernel(
    q_ref, k_ref, v_ref, qg_ref, kg_ref, sink_ref, gain_ref, ids_ref, rw_ref,
    tok_hbm, ow_hbm, wg_hbm, wu_hbm, wd_hbm, sg_hbm, su_hbm, sd_hbm,
    mix_out, exp_out,
    normed, ow, wg, wu, wd, sg, su, sd,
    slots, disp_send, disp_recv, rs_relay, rs_side, ret_send, ret_recv,
    mix_send, mix_relay, mix_side, sh_send, sh_relay, sh_side, acc, turn,
    halo, kd, vd, heads,
    load_sem, dsend, drecv, xsend, xrecv, tsend, trecv, hsend, hrecv,
):
    z, y, c, x = (lax.axis_index(a) for a in EP_TP)
    me = (z * NY + y) * NC + c

    def ep_peer(chunk, k, sign=1):
        dc, dz = chunk // 4, lax.rem(chunk + k, 4)
        if sign < 0:
            dz = NZ - dz
        return (lax.rem(z + dz, NZ), lax.rem(y + (k * sign) % NY, NY), lax.rem(c + dc, NC), x)

    def x_peer(d):
        return (z, y, c, lax.rem(x + d % N_TP, N_TP))

    barrier = pltpu.get_barrier_semaphore()
    for owner in range(1, N_EP):
        pl.semaphore_signal(
            barrier, inc=1, device_id=ep_peer(owner // 4, owner % 4), device_id_type=MESH_ID
        )
    for d in range(1, N_TP):
        pl.semaphore_signal(barrier, inc=1, device_id=x_peer(d), device_id_type=MESH_ID)

    loads = [
        pltpu.make_async_copy(s, t, load_sem.at[i])
        for i, (s, t) in enumerate(
            [(tok_hbm, normed), (sg_hbm, sg), (su_hbm, su), (sd_hbm, sd), (ow_hbm, ow),
             (wg_hbm, wg), (wu_hbm, wu), (wd_hbm, wd)]
        )
    ]
    loads[0].start()

    ids = ids_ref[...]
    expert = lax.broadcasted_iota(jnp.int32, (EXPERTS, ROWS), 0)
    first = (expert == ids[0:1, :]).astype(F32)
    second = (expert == ids[1:2, :]).astype(F32)
    s_row = lax.broadcasted_iota(jnp.int32, (ROWS, ROWS), 0)
    s_col = lax.broadcasted_iota(jnp.int32, (ROWS, ROWS), 1)
    earlier = ((s_row < s_col) & ((s_row >> 7) == (s_col >> 7))).astype(F32).astype(BF)
    seen = dot((first + second).astype(BF), earlier)
    rank_a = jnp.sum(first * seen, axis=0, keepdims=True)
    rank_b = jnp.sum(second * seen, axis=0, keepdims=True)
    owner = ids >> 2
    dy = ((owner >> 1) - y) & 3
    chunk_at = ((owner ^ c) & 1) * 4 + (((owner >> 3) - z - dy) & 3)
    block_at = lax.broadcasted_iota(jnp.int32, (2, ROWS), 1) >> 7
    rank = jnp.concatenate([rank_a, rank_b], axis=0)
    sent_at = chunk_at * CHUNK + (ids & 3) * 64 + dy * 16 + block_at * CAP
    back_at = chunk_at * QUARTER + dy * 16 + (ids & 3) * CAP
    slots[0:2, :] = sent_at.astype(F32) + rank
    slots[2:4, :] = back_at.astype(F32) + rank

    p_row = lax.broadcasted_iota(jnp.int32, (CHUNK, CHUNK), 0)
    p_col = lax.broadcasted_iota(jnp.int32, (CHUNK, CHUNK), 1)
    p_from = ((p_row >> 2) & 3) * 64 + ((p_row >> 4) & 3) * 16 + (p_row >> 6) * 4 + (p_row & 3)
    turn[...] = (p_from == p_col).astype(F32).astype(BF)

    with jax.named_scope('wait_tokens'):
        loads[0].wait()
    for cp in loads[1:]:
        cp.start()

    def norm_step(i, carry):
        rows = pl.ds(pl.multiple_of(i * 64, 64), 64)
        wide = normed[rows, :].astype(F32)
        scale = lax.rsqrt(jnp.mean(wide * wide, axis=-1, keepdims=True) + EPS)
        normed[rows, :] = ((wide * scale) * gain_ref[...]).astype(BF)
        return carry

    with jax.named_scope('norm'):
        lax.fori_loop(0, ROWS // 64, norm_step, 0)

    def slot_rows(base, shape):
        return (lax.broadcasted_iota(jnp.int32, shape, 0) + base).astype(F32)

    def send_chunk(i):
        for j in range(LOCAL):
            for k in range(4):
                rows = pl.ds(j * 64 + k * 16, 16)

                def start(rows=rows, k=k):
                    pltpu.make_async_remote_copy(
                        src_ref=disp_send.at[i, rows], dst_ref=disp_recv.at[i, rows],
                        send_sem=dsend.at[i], recv_sem=drecv.at[i],
                        device_id=ep_peer(i, k), device_id_type=MESH_ID,
                    ).start()

                if k:
                    start()
                else:
                    pl.when(i > 0)(start)

    def send_back(i):
        for k in range(4):
            rows = pl.ds(k * 16, 16)

            def start(rows=rows, k=k):
                pltpu.make_async_remote_copy(
                    src_ref=ret_send.at[i, rows], dst_ref=ret_recv.at[i, rows],
                    send_sem=tsend.at[i], recv_sem=trecv.at[i],
                    device_id=ep_peer(i, k, -1), device_id_type=MESH_ID,
                ).start()

            if k:
                start()
            else:
                pl.when(i > 0)(start)

    def wait_chunk(buf, to, i, send_sem, recv_sem):
        rows_in = buf.shape[1]

        def wait(count):
            rows = pl.ds(0, count)
            pltpu.make_async_remote_copy(
                src_ref=buf.at[i, rows], dst_ref=to.at[i, rows],
                send_sem=send_sem.at[i], recv_sem=recv_sem.at[i],
                device_id=ep_peer(0, 1), device_id_type=MESH_ID,
            ).wait()

        pl.when(i == 0)(lambda: wait(rows_in * 3 // 4))
        pl.when(i > 0)(lambda: wait(rows_in))

    nxt = lax.rem(me + 1, N_EP)
    nxt_dev = (nxt // (NY * NC), lax.rem(nxt // NC, NY), lax.rem(nxt, NC), x)
    halos = [
        pltpu.make_async_remote_copy(
            src_ref=ref.at[pl.ds(ROWS - BLOCK, BLOCK)], dst_ref=halo.at[i],
            send_sem=hsend.at[i], recv_sem=hrecv.at[i],
            device_id=nxt_dev, device_id_type=MESH_ID,
        )
        for i, ref in enumerate((k_ref, v_ref))
    ]

    def gather_step(i, carry):
        index = slot_rows(i * CHUNK, (CHUNK, ROWS))
        pick = (index == slots[0:1, :]) | (index == slots[1:2, :])
        pick = pick.astype(F32).astype(BF)
        for n in range(N_TP):
            cols = slice(n * COLS, (n + 1) * COLS)
            disp_send[i, :, cols] = dot(pick, normed[:, cols]).astype(BF)

        if carry is None:
            with jax.named_scope('barrier'):
                pl.semaphore_wait(barrier, N_EP - 1 + N_TP - 1)
            for cp in halos:
                cp.start()
        with jax.named_scope('send'):
            send_chunk(i)
        return carry

    gather_step(0, None)
    for j in range(LOCAL):
        rows = slice(j * 64, j * 64 + 16)
        disp_recv[0, rows, :] = disp_send[0, rows, :]


    def x_copy(t, n, src, dst, d):
        return pltpu.make_async_remote_copy(
            src_ref=src, dst_ref=dst, send_sem=xsend.at[t, n], recv_sem=xrecv.at[t, n],
            device_id=x_peer(d), device_id_type=MESH_ID,
        )

    def x_copies(which, t, part, relay, sides):
        routes = (
            (part(2, 0), relay(0), 1),
            (part(2, 1), relay(1), -1),
            (part(1, 1), sides(0, 1), 1),
            (part(-1, 0), sides(1, 0), -1),
            (part(1, 0), sides(0, 0), 1),
            (part(-1, 1), sides(1, 1), -1),
        )
        return [x_copy(t, n, *routes[n]) for n in which]

    def start_first(*refs):
        for cp in x_copies((0, 1, 2, 3), *refs):
            cp.start()

    def start_second(t, part, relay, sides):
        for cp in x_copies((0, 1), t, part, relay, sides):
            cp.wait()
        for n, d in ((0, 1), (1, -1)):
            own = part(d, n)
            own[...] = (own[...].astype(F32) + relay(n)[...].astype(F32)).astype(BF)
        for cp in x_copies((4, 5), t, part, relay, sides):
            cp.start()

    def wait_rest(*refs):
        for cp in x_copies((2, 3, 4, 5), *refs):
            cp.wait()

    def summed(t, part, relay, sides, half):
        return (
            part(0, half)[...].astype(F32)
            + sides(0, half)[...].astype(F32) + sides(1, half)[...].astype(F32)
        )

    def by_quarter(t, buf, rows_in, relay, side):
        half = rows_in // 2

        def part(d, n):
            at = lax.rem(x + d % N_TP, N_TP) * rows_in + n * half
            return buf.at[pl.ds(pl.multiple_of(at, half), half)]

        return (
            t, part, lambda n: relay.at[n],
            lambda s, n: side.at[s, pl.ds(n * half, half)],
        )

    def shared_refs():
        return by_quarter(CHUNKS, sh_send, BLOCK, sh_relay, sh_side)

    def mixer_refs():
        return by_quarter(CHUNKS + 1, mix_send, BLOCK, mix_relay, mix_side)

    def expert_refs(i):
        return by_quarter(i, disp_send.at[i], QUARTER, rs_relay.at[i], rs_side.at[i])

    for cp in loads[1:4]:
        cp.wait()
    gate = dot(normed[...], sg[...])
    up = dot(normed[...], su[...])
    hidden = (gate / (1.0 + jnp.exp(-gate)) * up).astype(BF)
    for n in range(N_TP):
        cols = slice(n * COLS, (n + 1) * COLS)
        sh_send[:, cols] = dot(hidden, sd[:, cols]).astype(BF)

    start_first(*shared_refs())
    with jax.named_scope('gather'):
        lax.fori_loop(1, CHUNKS, gather_step, 0)

    lane = lax.broadcasted_iota(jnp.int32, (1, 128), 1)
    low = lane < HEAD_DIM
    half_a = lax.broadcasted_iota(jnp.int32, (128, 128), 0) >> 6
    half_b = lax.broadcasted_iota(jnp.int32, (128, 128), 1) >> 6
    same_half = (half_a == half_b).astype(F32).astype(BF)

    q_gain = jnp.concatenate([qg_ref[...], qg_ref[...]], axis=1)
    k_gain = jnp.concatenate([kg_ref[...], kg_ref[...]], axis=1)

    def head_norm(rows_in, gain):
        wide = rows_in.astype(F32)
        square = wide * wide
        top = square.astype(BF)
        rest = (square - top.astype(F32)).astype(BF)
        total = dot(top, same_half) + dot(rest, same_half)
        scale = lax.rsqrt(total * (1.0 / HEAD_DIM) + EPS)
        return ((wide * scale) * gain).astype(BF)

    def both_halves(rows_in, dst, rows):
        wide = rows_in.astype(F32)
        turned = pltpu.roll(wide, HEAD_DIM, 1)
        dst[0, rows, :] = jnp.where(low, wide, turned).astype(BF)
        dst[1, rows, :] = jnp.where(low, turned, wide).astype(BF)

    own_rows = slice(BLOCK, BLOCK + ROWS)
    both_halves(head_norm(k_ref[...], k_gain), kd, own_rows)
    both_halves(v_ref[...], vd, own_rows)
    with jax.named_scope('halo_wait'):
        for cp in halos:
            cp.wait()
    both_halves(head_norm(halo[0], k_gain), kd, slice(0, BLOCK))
    both_halves(halo[1], vd, slice(0, BLOCK))
    query_pos = lax.broadcasted_iota(jnp.int32, (BLOCK, 2 * BLOCK), 0)
    key_pos = lax.broadcasted_iota(jnp.int32, (BLOCK, 2 * BLOCK), 1)

    def attend(n, carry):
        rows = pl.ds(pl.multiple_of(n * BLOCK, BLOCK), BLOCK)
        band = pl.ds(pl.multiple_of(n * BLOCK, BLOCK), 2 * BLOCK)
        floor = jnp.where(me * 4 + n == 0, BLOCK, 0)
        inside = (key_pos <= query_pos + BLOCK) & (key_pos > query_pos) & (key_pos >= floor)
        for kv in range(2):
            parts = []
            for b in range(2):
                cols = slice((kv * 2 + b) * 128, (kv * 2 + b + 1) * 128)
                qn = head_norm(q_ref[rows, cols], q_gain).astype(F32)
                parts.append(jnp.where(low, qn, 0.0).astype(BF))
                parts.append(jnp.where(low, 0.0, qn).astype(BF))
            stacked = jnp.concatenate(parts, axis=0)
            scores = lax.dot_general(
                stacked, kd[kv, band, :], (((1,), (1,)), ((), ())), preferred_element_type=F32
            ) * 0.125
            probs = []
            for g in range(4):
                sink = sink_ref[0, kv * 4 + g]
                part = jnp.where(inside, scores[g * BLOCK:(g + 1) * BLOCK], MASKED)
                top = jnp.maximum(jnp.max(part, axis=-1, keepdims=True), sink)
                ex = jnp.exp(part - top)
                den = jnp.sum(ex, axis=-1, keepdims=True) + jnp.exp(sink - top)
                probs.append((ex * (1.0 / den)).astype(BF))
            mixed = dot(jnp.concatenate(probs, axis=0), vd[kv, band, :])
            for b in range(2):
                lo = mixed[(2 * b) * BLOCK:(2 * b + 1) * BLOCK]
                hi = mixed[(2 * b + 1) * BLOCK:(2 * b + 2) * BLOCK]
                cols = slice((kv * 2 + b) * 128, (kv * 2 + b + 1) * 128)
                heads[rows, cols] = jnp.where(low, lo, hi).astype(BF)
        return carry

    with jax.named_scope('attend'):
        lax.fori_loop(0, ROWS // BLOCK, attend, 0)
    loads[4].wait()
    for n in range(N_TP):
        cols = slice(n * COLS, (n + 1) * COLS)
        mix_send[:, cols] = dot(heads[...], ow[:, cols]).astype(BF)

    start_first(*mixer_refs())
    with jax.named_scope('shared2'):
        start_second(*shared_refs())

    loads[5].wait()
    loads[6].wait()
    loads[7].wait()

    own_tokens = pl.ds(pl.multiple_of(x * BLOCK, BLOCK), BLOCK)

    def combine(i, carry):
        with jax.named_scope('wait_ret'):
            wait_chunk(ret_send, ret_recv, i, tsend, trecv)
        with jax.named_scope('combine'):
            index = slot_rows(i * QUARTER, (QUARTER, BLOCK))
            weight = jnp.where(index == slots[2:3, own_tokens], rw_ref[0:1, own_tokens], 0.0)
            weight += jnp.where(index == slots[3:4, own_tokens], rw_ref[1:2, own_tokens], 0.0)
            main = weight.astype(BF)
            rest = (weight - main.astype(F32)).astype(BF)
            dims = (((0,), (0,)), ((), ()))
            acc[...] += lax.dot_general(
                main, ret_recv[i], dims, preferred_element_type=F32
            ) + lax.dot_general(rest, ret_recv[i], dims, preferred_element_type=F32)
        return carry

    def step(i, carry):
        @pl.when(i < CHUNKS)
        def _():
            with jax.named_scope('wait_disp'):
                wait_chunk(disp_send, disp_recv, i, dsend, drecv)
            with jax.named_scope('ffn'):
                wide = []
                for j in range(LOCAL):
                    came = disp_recv[i, j * 64:(j + 1) * 64, :]
                    gate = dot(came, wg[j])
                    up = dot(came, wu[j])
                    hidden = (gate / (1.0 + jnp.exp(-gate)) * up).astype(BF)
                    wide.append(dot(turn[:, j * 64:(j + 1) * 64], hidden).astype(BF))
                wide = jnp.concatenate(wide, axis=1)
                for n in range(N_TP):
                    cols = slice(n * COLS, (n + 1) * COLS)
                    disp_send[i, :, cols] = dot(wide, wd[:, cols]).astype(BF)
            start_first(*expert_refs(i))

        @pl.when(i == 2)
        def _():
            with jax.named_scope('mix2'):
                start_second(*mixer_refs())

        @pl.when((i >= 1) & (i <= CHUNKS))
        def _():
            with jax.named_scope('rs2'):
                start_second(*expert_refs(i - 1))

        @pl.when(i == CHUNKS)
        def _():
            with jax.named_scope('mix_out'):
                wait_rest(*mixer_refs())
                for half in range(2):
                    rows = slice(half * BLOCK // 2, (half + 1) * BLOCK // 2)
                    mix_out[rows, :] = summed(*mixer_refs(), half).astype(BF)

        @pl.when((i >= 2) & (i <= CHUNKS + 1))
        def _():
            h = i - 2
            with jax.named_scope('wait_rs'):
                wait_rest(*expert_refs(h))
            with jax.named_scope('ret'):
                for half in range(2):
                    rows = slice(half * QUARTER // 2, (half + 1) * QUARTER // 2)
                    ret_send[h, rows, :] = summed(*expert_refs(h), half).astype(BF)
                send_back(h)

            @pl.when(h == 0)
            def _():
                ret_recv[0, 0:16, :] = ret_send[0, 0:16, :]

        @pl.when(i == 3)
        def _():
            with jax.named_scope('wait_shared'):
                wait_rest(*shared_refs())
            for half in range(2):
                rows = slice(half * BLOCK // 2, (half + 1) * BLOCK // 2)
                acc[rows, :] = summed(*shared_refs(), half).astype(BF).astype(F32)

        first_h = jnp.where(i <= CHUNKS, 0, jnp.where(i == CHUNKS + 1, 3, 7))
        last_h = jnp.where(i < CHUNKS, 0, jnp.where(i == CHUNKS, 3, jnp.where(i == CHUNKS + 1, 7, 8)))
        lax.fori_loop(first_h, last_h, combine, 0)
        return carry

    lax.fori_loop(0, CHUNKS + 3, step, 0)
    exp_out[...] = acc[...].astype(BF)


def hand_over(mix_in, exp_in, mix_out, exp_out):
    mix_out[...] = mix_in[...]
    exp_out[...] = exp_in[...]


def shards(
    query_rows, key_rows, value_rows, query_gain, key_gain, sink_logit, out_weight, tokens,
    norm_gain, expert_ids, route_weight, gate_weight, up_weight, down_weight,
    shared_gate, shared_up, shared_down,
):
    vmem = pl.BlockSpec(memory_space=pltpu.VMEM)
    hbm = pl.BlockSpec(memory_space=pl.ANY)
    smem = pl.BlockSpec(memory_space=pltpu.SMEM)
    dma = pltpu.SemaphoreType.DMA
    out = jax.ShapeDtypeStruct((BLOCK, D), BF)
    results = pl.pallas_call(
        layer_kernel,
        out_shape=(out, out),
        in_specs=[vmem] * 5 + [smem] + [vmem] * 3 + [hbm] * 8,
        out_specs=(vmem, vmem),
        scratch_shapes=[
            pltpu.VMEM((ROWS, D), BF),
            pltpu.VMEM((ROWS, D), BF),
            pltpu.VMEM((LOCAL, D, FFS), BF),
            pltpu.VMEM((LOCAL, D, FFS), BF),
            pltpu.VMEM((LOCAL * FFS, D), BF),
            pltpu.VMEM((D, FFS), BF),
            pltpu.VMEM((D, FFS), BF),
            pltpu.VMEM((FFS, D), BF),
            pltpu.VMEM((4, ROWS), F32),
            pltpu.VMEM((CHUNKS, CHUNK, D), BF),
            pltpu.VMEM((CHUNKS, CHUNK, D), BF),
            pltpu.VMEM((CHUNKS, 2, QUARTER // 2, D), BF),
            pltpu.VMEM((CHUNKS, 2, QUARTER, D), BF),
            pltpu.VMEM((CHUNKS, QUARTER, D), BF),
            pltpu.VMEM((CHUNKS, QUARTER, D), BF),
            pltpu.VMEM((ROWS, D), BF),
            pltpu.VMEM((2, BLOCK // 2, D), BF),
            pltpu.VMEM((2, BLOCK, D), BF),
            pltpu.VMEM((ROWS, D), BF),
            pltpu.VMEM((2, BLOCK // 2, D), BF),
            pltpu.VMEM((2, BLOCK, D), BF),
            pltpu.VMEM((BLOCK, D), F32),
            pltpu.VMEM((CHUNK, CHUNK), BF),
            pltpu.VMEM((2, BLOCK, 128), BF),
            pltpu.VMEM((2, BLOCK + ROWS, 128), BF),
            pltpu.VMEM((2, BLOCK + ROWS, 128), BF),
            pltpu.VMEM((ROWS, 512), BF),
            dma((8,)),
            dma((CHUNKS,)), dma((CHUNKS,)),
            dma((CHUNKS + 2, 6)), dma((CHUNKS + 2, 6)),
            dma((CHUNKS,)), dma((CHUNKS,)),
            dma((2,)), dma((2,)),
        ],
        compiler_params=pltpu.CompilerParams(
            collective_id=0, has_side_effects=True, vmem_limit_bytes=67000000
        ),
        name="layer",
    )(
        query_rows, key_rows, value_rows,
        query_gain[None], key_gain[None],
        sink_logit[None], norm_gain[None], expert_ids.T, route_weight.T,
        tokens, out_weight, gate_weight, up_weight, down_weight.reshape(LOCAL * FFS, D),
        shared_gate, shared_up, shared_down,
    )
    return tuple(
        pl.pallas_call(
            hand_over, out_shape=(out, out), in_specs=[vmem] * 2, out_specs=(vmem, vmem),
            name="hand_over",
        )(*results)
    )


def solution(mesh):
    split = Mesh(mesh.devices.reshape(NZ, NY, NC, mesh.shape["tp"]), EP_TP)
    return jax.shard_map(
        shards,
        mesh=split,
        in_specs=(
            P(EP, "x"), P(EP, "x"), P(EP, "x"), P(), P(), P("x"), P("x", None),
            P(EP, None), P(), P(EP, None), P(EP, None),
            P(EP, None, "x"), P(EP, None, "x"), P(EP, "x", None),
            P(None, "x"), P(None, "x"), P("x", None),
        ),
        out_specs=(P(EP_TP, None), P(EP_TP, None)),
        check_vma=False,
    )
```

time: 145 us -> 143 us (0.986)
  local copies, waits for them, and re-layouts: 3.76 us -> 0 us
    unnamed x2 -> x0, local copies, waits for them, and re-layouts: 3.76 us -> none
    pallas_call x0 -> x1, Pallas kernels: none -> 2.2 us  [shards(): pl.pallas_call(hand_over, out_shape=(out, out), in_specs=[vmem] * 2, out_...]
where the time goes in v2:
time: 143 us; the launch traced here: 142 us
  Pallas kernels  141 us (99%)
    pallas_call x1, Pallas kernels, shards(): pl.pallas_call(layer_kernel, out_shape=(out, out), in_specs=[vmem] * 5 +...  139 us

profile of v2, /device:TPU:1, one launch (start us, length us, event | category | flops | bytes accessed | tf_op | source)
XLA Modules:
  0.0 141.5 jit_solution(8868707208864991618)
XLA Ops:
  0.6 138.7 %layer.1 = (bf16[128,2048]{1,0:T(8,128)(2,1)}, bf16[128,2048]{1,0:T(8,128)(2,1)}) custom-call(bf16[512,512]{1,0:T(8,128)(2,1)} %q_ref.1, bf16[512,128]{1,0:T(8,128)(2,1)} %k_ref.1, bf16[512,128]{1,0:T(8,128)(2,1)} %v_ref.1, f32[1,64]{1,0:T(1,128)} %bitcast.11, f32[1,64]{1,0:T(1,128)} %bitcast.12, f32[1,8]{1,0:T(1,128)} %bitcast.13, f32[1,2048]{1,0:T(1,128)} %bitcast.8, ...), custom_call_target="tpu_custom_call" | custom-call | tf_op jit(solution)/shard_map/layer/pallas_call | solution.py:460
  139.3 2.2 %hand_over.1 = (bf16[128,2048]{1,0:T(8,128)(2,1)}, bf16[128,2048]{1,0:T(8,128)(2,1)}) custom-call(bf16[128,2048]{1,0:T(8,128)(2,1)} %get-tuple-element.4.mix_in, bf16[128,2048]{1,0:T(8,128)(2,1)} %get-tuple-element.5.exp_in), custom_call_target="tpu_custom_call" | custom-call | tf_op jit(solution)/shard_map/hand_over/pallas_call | solution.py:511

commit v3 on v2

--- a/solution.py
+++ b/solution.py
@@ -45,16 +45,21 @@
     slots, disp_send, disp_recv, rs_relay, rs_side, ret_send, ret_recv,
     mix_send, mix_relay, mix_side, sh_send, sh_relay, sh_side, acc, turn,
     halo, kd, vd, heads,
-    load_sem, dsend, drecv, xsend, xrecv, tsend, trecv, hsend, hrecv,
+    load_sem, dsend, drecv, gsend, grecv, xsend, xrecv, tsend, trecv, hsend, hrecv,
 ):
     z, y, c, x = (lax.axis_index(a) for a in EP_TP)
     me = (z * NY + y) * NC + c
 
     def ep_peer(chunk, k, sign=1):
-        dc, dz = chunk // 4, lax.rem(chunk + k, 4)
+        g, dc = lax.rem(chunk, 4), chunk // 4
+        latin = (g + 3) // 4
+        both = 2 * (k // 2) + dc
+        dy = latin * k + (1 - latin) * both
+        dz = latin * lax.rem(g + k, 4) + (1 - latin) * both
+        dc = latin * dc + (1 - latin) * (k % 2)
         if sign < 0:
-            dz = NZ - dz
-        return (lax.rem(z + dz, NZ), lax.rem(y + (k * sign) % NY, NY), lax.rem(c + dc, NC), x)
+            dy, dz = NY - dy, NZ - dz
+        return (lax.rem(z + dz, NZ), lax.rem(y + dy, NY), lax.rem(c + dc, NC), x)
 
     def x_peer(d):
         return (z, y, c, lax.rem(x + d % N_TP, N_TP))
@@ -88,11 +93,17 @@
     rank_b = jnp.sum(second * seen, axis=0, keepdims=True)
     owner = ids >> 2
     dy = ((owner >> 1) - y) & 3
-    chunk_at = ((owner ^ c) & 1) * 4 + (((owner >> 3) - z - dy) & 3)
+    dc = (owner ^ c) & 1
+    g = ((owner >> 3) - z - dy) & 3
+    chunk_at = jnp.where(g == 0, (dy & 1) * 4, dc * 4 + g)
+    k_at = jnp.where(g == 0, (dy >> 1) * 2 + dc, dy)
     block_at = lax.broadcasted_iota(jnp.int32, (2, ROWS), 1) >> 7
     rank = jnp.concatenate([rank_a, rank_b], axis=0)
-    sent_at = chunk_at * CHUNK + (ids & 3) * 64 + dy * 16 + block_at * CAP
-    back_at = chunk_at * QUARTER + dy * 16 + (ids & 3) * CAP
+    sent_at = chunk_at * CHUNK + (ids & 3) * 64 + k_at * 16 + block_at * CAP
+    sent_at = jnp.where(
+        chunk_at == 0, block_at * QUARTER + k_at * 16 + (ids & 3) * CAP, sent_at
+    )
+    back_at = chunk_at * QUARTER + k_at * 16 + (ids & 3) * CAP
     slots[0:2, :] = sent_at.astype(F32) + rank
     slots[2:4, :] = back_at.astype(F32) + rank
 
@@ -119,22 +130,57 @@
     def slot_rows(base, shape):
         return (lax.broadcasted_iota(jnp.int32, shape, 0) + base).astype(F32)
 
+    def send_rows(i, k, rows):
+        pltpu.make_async_remote_copy(
+            src_ref=disp_send.at[i, rows], dst_ref=disp_recv.at[i, rows],
+            send_sem=dsend.at[i], recv_sem=drecv.at[i],
+            device_id=ep_peer(i, k), device_id_type=MESH_ID,
+        ).start()
+
     def send_chunk(i):
         for j in range(LOCAL):
             for k in range(4):
-                rows = pl.ds(j * 64 + k * 16, 16)
-
-                def start(rows=rows, k=k):
-                    pltpu.make_async_remote_copy(
-                        src_ref=disp_send.at[i, rows], dst_ref=disp_recv.at[i, rows],
-                        send_sem=dsend.at[i], recv_sem=drecv.at[i],
-                        device_id=ep_peer(i, k), device_id_type=MESH_ID,
-                    ).start()
-
-                if k:
-                    start()
-                else:
-                    pl.when(i > 0)(start)
+                send_rows(i, k, pl.ds(j * 64 + k * 16, 16))
+
+    def send_own_quarter():
+        for n in range(N_TP):
+            rows = pl.ds(n * QUARTER + 16, 16)
+            pltpu.make_async_remote_copy(
+                src_ref=disp_send.at[0, rows], dst_ref=disp_recv.at[0, rows],
+                send_sem=gsend.at[4 + n], recv_sem=grecv.at[4 + n],
+                device_id=ep_peer(0, 1), device_id_type=MESH_ID,
+            ).start()
+        for k in range(2, 4):
+            send_rows(0, k, pl.ds(pl.multiple_of(x * QUARTER + k * 16, 16), 16))
+
+    def wait_partner():
+        for n in range(N_TP):
+            rows = pl.ds(n * QUARTER + 16, 16)
+            pltpu.make_async_remote_copy(
+                src_ref=disp_send.at[0, rows], dst_ref=disp_recv.at[0, rows],
+                send_sem=gsend.at[4 + n], recv_sem=grecv.at[4 + n],
+                device_id=ep_peer(0, 1), device_id_type=MESH_ID,
+            ).wait()
+
+    def pass_on(which):
+        halves = (slice(0, D // 2), slice(D // 2, D))
+
+        def at(d, cols):
+            first = lax.rem(x + d % N_TP, N_TP) * QUARTER + 32
+            return disp_recv.at[0, pl.ds(pl.multiple_of(first, 32), 32), cols]
+
+        routes = (
+            (at(0, slice(0, D)), 1), (at(0, slice(0, D)), -1),
+            (at(-1, halves[0]), 1), (at(1, halves[1]), -1),
+        )
+        return [
+            pltpu.make_async_remote_copy(
+                src_ref=routes[n][0], dst_ref=routes[n][0],
+                send_sem=gsend.at[n], recv_sem=grecv.at[n],
+                device_id=x_peer(routes[n][1]), device_id_type=MESH_ID,
+            )
+            for n in which
+        ]
 
     def send_back(i):
         for k in range(4):
@@ -152,19 +198,20 @@
             else:
                 pl.when(i > 0)(start)
 
-    def wait_chunk(buf, to, i, send_sem, recv_sem):
-        rows_in = buf.shape[1]
-
-        def wait(count):
-            rows = pl.ds(0, count)
-            pltpu.make_async_remote_copy(
-                src_ref=buf.at[i, rows], dst_ref=to.at[i, rows],
-                send_sem=send_sem.at[i], recv_sem=recv_sem.at[i],
-                device_id=ep_peer(0, 1), device_id_type=MESH_ID,
-            ).wait()
-
-        pl.when(i == 0)(lambda: wait(rows_in * 3 // 4))
-        pl.when(i > 0)(lambda: wait(rows_in))
+    def wait_rows(buf, to, i, send_sem, recv_sem, count):
+        rows = pl.ds(0, count)
+        pltpu.make_async_remote_copy(
+            src_ref=buf.at[i, rows], dst_ref=to.at[i, rows],
+            send_sem=send_sem.at[i], recv_sem=recv_sem.at[i],
+            device_id=ep_peer(0, 1), device_id_type=MESH_ID,
+        ).wait()
+
+    def wait_chunk(i, count):
+        wait_rows(disp_send, disp_recv, i, dsend, drecv, count)
+
+    def wait_back(i):
+        pl.when(i == 0)(lambda: wait_rows(ret_send, ret_recv, i, tsend, trecv, QUARTER - 16))
+        pl.when(i > 0)(lambda: wait_rows(ret_send, ret_recv, i, tsend, trecv, QUARTER))
 
     nxt = lax.rem(me + 1, N_EP)
     nxt_dev = (nxt // (NY * NC), lax.rem(nxt // NC, NY), lax.rem(nxt, NC), x)
@@ -190,15 +237,16 @@
                 pl.semaphore_wait(barrier, N_EP - 1 + N_TP - 1)
             for cp in halos:
                 cp.start()
-        with jax.named_scope('send'):
+            send_own_quarter()
+        else:
             send_chunk(i)
         return carry
 
     gather_step(0, None)
-    for j in range(LOCAL):
-        rows = slice(j * 64, j * 64 + 16)
+    lax.fori_loop(1, 2, gather_step, 0)
+    for n in range(N_TP):
+        rows = slice(n * QUARTER, n * QUARTER + 16)
         disp_recv[0, rows, :] = disp_send[0, rows, :]
-
 
     def x_copy(t, n, src, dst, d):
         return pltpu.make_async_remote_copy(
@@ -270,9 +318,21 @@
         cols = slice(n * COLS, (n + 1) * COLS)
         sh_send[:, cols] = dot(hidden, sd[:, cols]).astype(BF)
 
-    start_first(*shared_refs())
+    for cp in x_copies((2, 3), *shared_refs()):
+        cp.start()
+    with jax.named_scope('own_quarter'):
+        wait_chunk(0, 32)
+    for cp in pass_on((0, 1)):
+        cp.start()
     with jax.named_scope('gather'):
-        lax.fori_loop(1, CHUNKS, gather_step, 0)
+        lax.fori_loop(2, CHUNKS, gather_step, 0)
+    with jax.named_scope('pass_on'):
+        for cp in pass_on((0, 1)):
+            cp.wait()
+    for cp in pass_on((2, 3)):
+        cp.start()
+    for cp in x_copies((0, 1), *shared_refs()):
+        cp.start()
 
     lane = lax.broadcasted_iota(jnp.int32, (1, 128), 1)
     low = lane < HEAD_DIM
@@ -360,7 +420,7 @@
 
     def combine(i, carry):
         with jax.named_scope('wait_ret'):
-            wait_chunk(ret_send, ret_recv, i, tsend, trecv)
+            wait_back(i)
         with jax.named_scope('combine'):
             index = slot_rows(i * QUARTER, (QUARTER, BLOCK))
             weight = jnp.where(index == slots[2:3, own_tokens], rw_ref[0:1, own_tokens], 0.0)
@@ -377,7 +437,17 @@
         @pl.when(i < CHUNKS)
         def _():
             with jax.named_scope('wait_disp'):
-                wait_chunk(disp_send, disp_recv, i, dsend, drecv)
+                pl.when(i > 0)(lambda: wait_chunk(i, CHUNK))
+
+                @pl.when(i == 0)
+                def _():
+                    for cp in pass_on((2, 3)):
+                        cp.wait()
+                    wait_partner()
+                    for n in range(N_TP):
+                        cols = slice(n * COLS, (n + 1) * COLS)
+                        disp_recv[0, :, cols] = dot(turn[...], disp_recv[0, :, cols]).astype(BF)
+
             with jax.named_scope('ffn'):
                 wide = []
                 for j in range(LOCAL):
@@ -390,7 +460,6 @@
                 for n in range(N_TP):
                     cols = slice(n * COLS, (n + 1) * COLS)
                     disp_send[i, :, cols] = dot(wide, wd[:, cols]).astype(BF)
-            start_first(*expert_refs(i))
 
         @pl.when(i == 2)
         def _():
@@ -401,6 +470,10 @@
         def _():
             with jax.named_scope('rs2'):
                 start_second(*expert_refs(i - 1))
+
+        @pl.when(i < CHUNKS)
+        def _():
+            start_first(*expert_refs(i))
 
         @pl.when(i == CHUNKS)
         def _():
@@ -492,6 +565,7 @@
             pltpu.VMEM((ROWS, 512), BF),
             dma((8,)),
             dma((CHUNKS,)), dma((CHUNKS,)),
+            dma((8,)), dma((8,)),
             dma((CHUNKS + 2, 6)), dma((CHUNKS + 2, 6)),
             dma((CHUNKS,)), dma((CHUNKS,)),
             dma((2,)), dma((2,)),

time: 143 us -> 136 us (0.951)
  Pallas kernels: 141 us -> 135 us
    pallas_call x1, Pallas kernels: 139 us -> 133 us  [shards(): pl.pallas_call(layer_kernel, out_shape=(out, out), in_specs=[vmem] * 5 +...]
where the time goes in v3:
time: 136 us
  Pallas kernels  135 us (99%)
    pallas_call x1, Pallas kernels, shards(): pl.pallas_call(layer_kernel, out_shape=(out, out), in_specs=[vmem] * 5 +...  133 us

profile of v3, /device:TPU:1, one launch (start us, length us, event | category | flops | bytes accessed | tf_op | source)
XLA Modules:
  0.0 135.6 jit_solution(4979109785654789375)
XLA Ops:
  0.6 132.8 %layer.1 = (bf16[128,2048]{1,0:T(8,128)(2,1)}, bf16[128,2048]{1,0:T(8,128)(2,1)}) custom-call(bf16[512,512]{1,0:T(8,128)(2,1)} %q_ref.1, bf16[512,128]{1,0:T(8,128)(2,1)} %k_ref.1, bf16[512,128]{1,0:T(8,128)(2,1)} %v_ref.1, f32[1,64]{1,0:T(1,128)} %bitcast.11, f32[1,64]{1,0:T(1,128)} %bitcast.12, f32[1,8]{1,0:T(1,128)} %bitcast.13, f32[1,2048]{1,0:T(1,128)} %bitcast.8, ...), custom_call_target="tpu_custom_call" | custom-call | tf_op jit(solution)/shard_map/layer/pallas_call | solution.py:533
  133.4 2.2 %hand_over.1 = (bf16[128,2048]{1,0:T(8,128)(2,1)}, bf16[128,2048]{1,0:T(8,128)(2,1)}) custom-call(bf16[128,2048]{1,0:T(8,128)(2,1)} %get-tuple-element.4.mix_in, bf16[128,2048]{1,0:T(8,128)(2,1)} %get-tuple-element.5.exp_in), custom_call_target="tpu_custom_call" | custom-call | tf_op jit(solution)/shard_map/hand_over/pallas_call | solution.py:585

commit v4 on v3

--- a/solution.py
+++ b/solution.py
@@ -320,20 +320,6 @@
 
     for cp in x_copies((2, 3), *shared_refs()):
         cp.start()
-    with jax.named_scope('own_quarter'):
-        wait_chunk(0, 32)
-    for cp in pass_on((0, 1)):
-        cp.start()
-    with jax.named_scope('gather'):
-        lax.fori_loop(2, CHUNKS, gather_step, 0)
-    with jax.named_scope('pass_on'):
-        for cp in pass_on((0, 1)):
-            cp.wait()
-    for cp in pass_on((2, 3)):
-        cp.start()
-    for cp in x_copies((0, 1), *shared_refs()):
-        cp.start()
-
     lane = lax.broadcasted_iota(jnp.int32, (1, 128), 1)
     low = lane < HEAD_DIM
     half_a = lax.broadcasted_iota(jnp.int32, (128, 128), 0) >> 6
@@ -403,6 +389,20 @@
 
     with jax.named_scope('attend'):
         lax.fori_loop(0, ROWS // BLOCK, attend, 0)
+    with jax.named_scope('own_quarter'):
+        wait_chunk(0, 32)
+    for cp in pass_on((0, 1)):
+        cp.start()
+    with jax.named_scope('gather'):
+        lax.fori_loop(2, CHUNKS, gather_step, 0)
+    with jax.named_scope('pass_on'):
+        for cp in pass_on((0, 1)):
+            cp.wait()
+    for cp in pass_on((2, 3)):
+        cp.start()
+    for cp in x_copies((0, 1), *shared_refs()):
+        cp.start()
+
     loads[4].wait()
     for n in range(N_TP):
         cols = slice(n * COLS, (n + 1) * COLS)
@@ -475,14 +475,6 @@
         def _():
             start_first(*expert_refs(i))
 
-        @pl.when(i == CHUNKS)
-        def _():
-            with jax.named_scope('mix_out'):
-                wait_rest(*mixer_refs())
-                for half in range(2):
-                    rows = slice(half * BLOCK // 2, (half + 1) * BLOCK // 2)
-                    mix_out[rows, :] = summed(*mixer_refs(), half).astype(BF)
-
         @pl.when((i >= 2) & (i <= CHUNKS + 1))
         def _():
             h = i - 2
@@ -506,8 +498,16 @@
                 rows = slice(half * BLOCK // 2, (half + 1) * BLOCK // 2)
                 acc[rows, :] = summed(*shared_refs(), half).astype(BF).astype(F32)
 
-        first_h = jnp.where(i <= CHUNKS, 0, jnp.where(i == CHUNKS + 1, 3, 7))
-        last_h = jnp.where(i < CHUNKS, 0, jnp.where(i == CHUNKS, 3, jnp.where(i == CHUNKS + 1, 7, 8)))
+        @pl.when(i == CHUNKS + 1)
+        def _():
+            with jax.named_scope('mix_out'):
+                wait_rest(*mixer_refs())
+                for half in range(2):
+                    rows = slice(half * BLOCK // 2, (half + 1) * BLOCK // 2)
+                    mix_out[rows, :] = summed(*mixer_refs(), half).astype(BF)
+
+        first_h = jnp.where(i <= CHUNKS + 1, 0, 7)
+        last_h = jnp.where(i < CHUNKS + 1, 0, jnp.where(i == CHUNKS + 1, 7, 8))
         lax.fori_loop(first_h, last_h, combine, 0)
         return carry
 
@@ -515,9 +515,21 @@
     exp_out[...] = acc[...].astype(BF)
 
 
-def hand_over(mix_in, exp_in, mix_out, exp_out):
-    mix_out[...] = mix_in[...]
-    exp_out[...] = exp_in[...]
+def hand_over(mix_in, exp_in, mix_out, exp_out, held, in_sem, out_sem):
+    pairs = [(src, dst, n) for n in range(2) for src, dst in ((mix_in, mix_out), (exp_in, exp_out))]
+    half = BLOCK // 2
+    copies_in, copies_out = [], []
+    for at, (src, dst, n) in enumerate(pairs):
+        rows = pl.ds(n * half, half)
+        copies_in.append(pltpu.make_async_copy(src.at[rows], held.at[at], in_sem.at[at]))
+        copies_out.append(pltpu.make_async_copy(held.at[at], dst.at[rows], out_sem.at[at]))
+    for cp in copies_in:
+        cp.start()
+    for got, put in zip(copies_in, copies_out):
+        got.wait()
+        put.start()
+    for cp in copies_out:
+        cp.wait()
 
 
 def shards(
@@ -583,7 +595,8 @@
     )
     return tuple(
         pl.pallas_call(
-            hand_over, out_shape=(out, out), in_specs=[vmem] * 2, out_specs=(vmem, vmem),
+            hand_over, out_shape=(out, out), in_specs=[hbm] * 2, out_specs=(hbm, hbm),
+            scratch_shapes=[pltpu.VMEM((4, BLOCK // 2, D), BF), dma((4,)), dma((4,))],
             name="hand_over",
         )(*results)
     )

time: 136 us -> 135 us (level)
  no operation moved by 1% of the time
where the time goes in v4:
time: 135 us
  Pallas kernels  134 us (99%)
    pallas_call x1, Pallas kernels, shards(): pl.pallas_call(layer_kernel, out_shape=(out, out), in_specs=[vmem] * 5 +...  133 us

profile of v4, /device:TPU:1, one launch (start us, length us, event | category | flops | bytes accessed | tf_op | source)
XLA Modules:
  0.0 135.1 jit_solution(10156841512266368822)
XLA Ops:
  0.6 132.5 %layer.1 = (bf16[128,2048]{1,0:T(8,128)(2,1)}, bf16[128,2048]{1,0:T(8,128)(2,1)}) custom-call(bf16[512,512]{1,0:T(8,128)(2,1)} %q_ref.1, bf16[512,128]{1,0:T(8,128)(2,1)} %k_ref.1, bf16[512,128]{1,0:T(8,128)(2,1)} %v_ref.1, f32[1,64]{1,0:T(1,128)} %bitcast.11, f32[1,64]{1,0:T(1,128)} %bitcast.12, f32[1,8]{1,0:T(1,128)} %bitcast.13, f32[1,2048]{1,0:T(1,128)} %bitcast.8, ...), custom_call_target="tpu_custom_call" | custom-call | tf_op jit(solution)/shard_map/layer/pallas_call | solution.py:545
  133.2 2.0 %hand_over.1 = (bf16[128,2048]{1,0:T(8,128)(2,1)}, bf16[128,2048]{1,0:T(8,128)(2,1)}) custom-call(bf16[128,2048]{1,0:T(8,128)(2,1)} %get-tuple-element.4.mix_in, bf16[128,2048]{1,0:T(8,128)(2,1)} %get-tuple-element.5.exp_in), custom_call_target="tpu_custom_call" | custom-call | tf_op jit(solution)/shard_map/hand_over/pallas_call | solution.py:597
